TPU v7x, 32 devices: a whole 2x2x4 slice. The times are simulated.
32 devices in a mesh: ep: 8 (over z, x), tp: 4 (over y, core).
Axes of the slice: x: 2, y: 2, z: 4, core: 2. Of those that a mesh axis runs over, the one named last changes fastest.
Arguments:
- tokens: bfloat16 [2048, 2048], P('ep'), may hold values from -6 to 6
- routes: int32 [2048, 4], P('ep'), may hold values from 0 to 7, all different within a row; in each aligned block of 256 rows (0 to 255, 256 to 511, ...) at most 160 rows name the same one
- gate_weights: float32 [2048, 4], P('ep'), may hold values from 0.05 to 1
- out_grad: bfloat16 [2048, 2048], P('ep'), may hold values from -0.59765625 to 0.59765625
- w_gate: bfloat16 [8, 2048, 1024], P('ep', None, 'tp'), may hold values from -0.1875 to 0.1875
- w_up: bfloat16 [8, 2048, 1024], P('ep', None, 'tp'), may hold values from -0.1875 to 0.1875
- w_down: bfloat16 [8, 1024, 2048], P('ep', 'tp'), may hold values from -0.1875 to 0.1875
Outputs:
- token_grad: bfloat16 [2048, 2048], P('ep', 'tp')
- gate_grad: float32 [2048, 4], P('ep')
- gate_weight_grad: float32 [8, 2048, 1024], P('ep', None, 'tp')
- up_weight_grad: float32 [8, 2048, 1024], P('ep', None, 'tp')
- down_weight_grad: float32 [8, 1024, 2048], P('ep', 'tp')
Inputs may be any that keep to these rules, and one draw needn't show every extreme that they name: `routes`: each row names 4 different experts. In each aligned block of 256 rows (the rows of one device) no expert is named by more than 160 rows, and in some block an expert is named by exactly 160 rows.
All inputs are finite; a program needn't handle non-finite values.
Results may differ from a plain program's by a relative error of at most 0.012.
Values may be sent and summed in bfloat16 or wider, within the bound.
A program may use at most 128 MiB of HBM per device.

v0:
```python
import jax
import jax.numpy as jnp
from jax import lax
from jax.sharding import PartitionSpec as P

clamp_limit = 7.0
sigmoid_slope = 1.702


def unit_backward(gate_pre, up_pre, hidden_grad):
    glu = jnp.minimum(gate_pre, clamp_limit)
    linear = jnp.clip(up_pre, -clamp_limit, clamp_limit)
    sigma = jax.nn.sigmoid(sigmoid_slope * glu)
    active = glu * sigma
    hidden = (active * (linear + 1.0)).astype(jnp.bfloat16)
    slope_term = sigma + sigmoid_slope * active * (1.0 - sigma)
    gate_pre_grad = jnp.where(
        gate_pre < clamp_limit, hidden_grad * (linear + 1.0) * slope_term, 0.0
    ).astype(jnp.bfloat16)
    up_pre_grad = jnp.where(jnp.abs(up_pre) < clamp_limit, hidden_grad * active, 0.0).astype(
        jnp.bfloat16
    )
    return (hidden, gate_pre_grad, up_pre_grad)


def local(tokens, routes, gate_weights, out_grad, w_gate, w_up, w_down):
    ep_count = lax.axis_size("ep")
    tp_count = lax.axis_size("tp")
    tp_index = lax.axis_index("tp")
    token_count, model_width = tokens.shape
    top_count = routes.shape[1]
    expert_local = w_gate.shape[0]
    experts_all = ep_count * expert_local
    capacity = token_count * top_count * 5 // (4 * experts_all)
    pair_count = token_count * top_count
    width_cols = model_width // tp_count
    flat_routes = routes.reshape(-1)
    onehot = (flat_routes[:, None] == jnp.arange(experts_all, dtype=jnp.int32)[None, :]).astype(
        jnp.int32
    )
    slot_rank = jnp.sum((jnp.cumsum(onehot, axis=0) - onehot) * onehot, axis=1)
    target = flat_routes * capacity + slot_rank
    pair_index = jnp.arange(pair_count, dtype=jnp.int32)
    pair_table = jnp.zeros((experts_all * capacity,), jnp.int32).at[target].set(pair_index)
    is_live = jnp.zeros((experts_all * capacity,), jnp.int32).at[target].set(1) > 0
    token_index = pair_table // top_count
    flat_weights = gate_weights.reshape(-1)
    live_column = is_live[:, None]
    send_rows = jnp.where(live_column, tokens[token_index], jnp.zeros((), jnp.bfloat16))
    send_grads = jnp.where(live_column, out_grad[token_index], jnp.zeros((), jnp.bfloat16))
    send_weights = jnp.where(is_live, flat_weights[pair_table], 0.0)
    col_start = tp_index * width_cols
    part_rows = lax.dynamic_slice_in_dim(send_rows, col_start, width_cols, 1)
    part_grads = lax.dynamic_slice_in_dim(send_grads, col_start, width_cols, 1)
    part_rows, part_grads = (
        lax.all_to_all(part_rows, "ep", split_axis=0, concat_axis=0, tiled=True),
        lax.all_to_all(part_grads, "ep", split_axis=0, concat_axis=0, tiled=True),
    )
    arrived, arrived_grads = (
        lax.all_gather(part_rows, "tp", axis=1, tiled=True),
        lax.all_gather(part_grads, "tp", axis=1, tiled=True),
    )
    arrived_weights = lax.all_to_all(send_weights, "ep", split_axis=0, concat_axis=0, tiled=True)
    row_count = ep_count * capacity
    grouped_rows = arrived.reshape(ep_count, expert_local, capacity, model_width)
    grouped_grads = arrived_grads.reshape(ep_count, expert_local, capacity, model_width)
    grouped_weights = arrived_weights.reshape(ep_count, expert_local, capacity)
    gate_grads, up_grads, down_grads, row_terms, product_terms = ([], [], [], [], [])
    x_rows = grouped_rows[:, 0].reshape(row_count, model_width)
    dy_rows = grouped_grads[:, 0].reshape(row_count, model_width)
    slot_weights = grouped_weights[:, 0].reshape(row_count, 1)
    scaled = (slot_weights * dy_rows.astype(jnp.float32)).astype(jnp.bfloat16)
    gate_pre = jnp.dot(x_rows, w_gate[0], preferred_element_type=jnp.float32)
    up_pre = jnp.dot(x_rows, w_up[0], preferred_element_type=jnp.float32)
    hidden_grad = jnp.einsum("rd,fd->rf", scaled, w_down[0], preferred_element_type=jnp.float32)
    hidden, gate_pre_grad, up_pre_grad = unit_backward(gate_pre, up_pre, hidden_grad)
    gate_grads.append(
        jnp.einsum("rd,rf->df", x_rows, gate_pre_grad, preferred_element_type=jnp.float32)
    )
    up_grads.append(
        jnp.einsum("rd,rf->df", x_rows, up_pre_grad, preferred_element_type=jnp.float32)
    )
    down_grads.append(jnp.einsum("rf,rd->fd", hidden, scaled, preferred_element_type=jnp.float32))
    row_term = jnp.einsum("rf,df->rd", gate_pre_grad, w_gate[0], preferred_element_type=jnp.float32)
    row_term = row_term + jnp.einsum(
        "rf,df->rd", up_pre_grad, w_up[0], preferred_element_type=jnp.float32
    )
    row_terms.append(row_term.astype(jnp.bfloat16).reshape(ep_count, capacity, model_width))
    out_term = jnp.dot(hidden, w_down[0], preferred_element_type=jnp.float32).astype(jnp.bfloat16)
    product = jnp.sum(dy_rows.astype(jnp.float32) * out_term.astype(jnp.float32), axis=1)
    product_terms.append(product.reshape(ep_count, capacity))
    all_rows = jnp.stack(row_terms, axis=1).reshape(experts_all * capacity, model_width)
    all_products = jnp.stack(product_terms, axis=1).reshape(experts_all * capacity)
    row_sum = lax.psum_scatter(all_rows, "tp", scatter_dimension=1, tiled=True).astype(jnp.float32)
    product_sum = lax.psum(all_products, "tp")
    back_rows = lax.all_to_all(
        row_sum.astype(jnp.bfloat16), "ep", split_axis=0, concat_axis=0, tiled=True
    )
    back_products = lax.all_to_all(product_sum, "ep", split_axis=0, concat_axis=0, tiled=True)
    pair_rows = back_rows[target].reshape(token_count, top_count, width_cols)
    token_grad = jnp.sum(pair_rows.astype(jnp.float32), axis=1).astype(jnp.bfloat16)
    gate_grad = back_products[target].reshape(token_count, top_count)
    return (
        token_grad,
        gate_grad,
        jnp.stack(gate_grads),
        jnp.stack(up_grads),
        jnp.stack(down_grads),
    )


def solution(mesh):
    return jax.shard_map(
        local,
        mesh=mesh,
        in_specs=(
            P("ep", None),
            P("ep", None),
            P("ep", None),
            P("ep", None),
            P("ep", None, "tp"),
            P("ep", None, "tp"),
            P("ep", "tp", None),
        ),
        out_specs=(
            P("ep", "tp"),
            P("ep", None),
            P("ep", None, "tp"),
            P("ep", None, "tp"),
            P("ep", "tp", None),
        ),
        check_vma=False,
    )
```

profile of v0, /device:TPU:11, one launch (start us, length us, event | category | flops | bytes accessed | tf_op | source)
XLA Modules:
  0.0 270.6 jit_solution(15589261127671438414)
XLA Ops:
  7.2 0.0 copy-start
  7.2 0.0 copy-start.1
  7.2 0.0 all-gather.3.cloned.1.call-start
  7.2 0.8 broadcast_multiply_fusion
  8.1 0.8 copy.18
  8.9 0.1 eq.29
  9.0 0.1 eq.25
  9.1 0.1 copy.17
  9.3 0.1 mul.61
  9.4 2.3 reduce-window.6
  11.7 0.3 slice_reduce_fusion
  12.0 0.2 reduce-window.9
  12.1 0.1 add_bitcast_fusion
  12.3 4.3 %scatter_custom_fusion.1 = s32[1280]{0:T(1024)S(1)} fusion(s32[1024]{0:T(1024)S(1)} %bitcast.69, s32[1024]{0:T(1024)S(1)} %iota.11, s32[]{:T(128)} %constant.18.clone.1), kind=kCustom, calls=%fused_computation.57 | custom fusion | bytes 5124 | tf_op jit(solution)/shard_map/scatter | solution.py:44
  16.6 4.3 %scatter_custom_fusion = s32[1280]{0:T(1024)S(1)} fusion(s32[1024]{0:T(1024)S(1)} %bitcast.70, s32[1024]{0:T(1024)S(1)} %broadcast.76, s32[]{:T(128)} %constant.18.clone.1), kind=kCustom, calls=%fused_computation.60 | custom fusion | bytes 5124 | tf_op jit(solution)/shard_map/scatter | solution.py:45
  21.0 0.8 copy.20
  21.8 0.1 reshape.79
  21.9 0.0 copy-done.1
  21.9 0.0 copy-start.2
  21.9 6.1 %gather_fusion.2 = bf16[1280,2048]{1,0:T(8,128)(2,1)} fusion(bf16[256,2048]{1,0:T(8,128)(2,1)S(1)} %copy-done.1, s32[2048]{0:T(1024)S(1)} %get-tuple-element.25), kind=kCustom, calls=%fused_computation.2 | custom fusion | bytes 10490880 | tf_op jit(solution)/shard_map/gather | solution.py:50
  28.1 0.0 copy-done.2
  28.1 6.1 %gather_fusion = bf16[1280,2048]{1,0:T(8,128)(2,1)} fusion(bf16[256,2048]{1,0:T(8,128)(2,1)S(1)} %copy-done.2, s32[2048]{0:T(1024)S(1)} %get-tuple-element.25), kind=kCustom, calls=%fused_computation | custom fusion | bytes 10490880 | tf_op jit(solution)/shard_map/gather | solution.py:49
  34.2 5.0 %gather_fusion.1 = f32[1280]{0:T(1024)S(1)} fusion(f32[1024]{0:T(1024)S(1)} %reshape.79, s32[2048]{0:T(1024)S(1)} %get-tuple-element.24), kind=kCustom, calls=%fused_computation.1 | custom fusion | bytes 15360 | tf_op jit(solution)/shard_map/gather | solution.py:51
  39.2 2.2 dynamic-slice_select_fusion.1
  41.4 0.0 copy-start.3
  41.4 34.0 %all_to_all.58 = bf16[8,160,512]{2,1,0:T(8,128)(2,1)} all-to-all(bf16[8,160,512]{2,1,0:T(8,128)(2,1)S(1)} %bitcast.64), channel_id=1, replica_groups=mesh['ep'=8,'tp'=4] {'ep'}, dimensions={0} | all-to-all | bytes 2621440 | tf_op jit(solution)/shard_map/all_to_all | solution.py:56
  75.4 0.0 all-gather.3.cloned.1.call-update
  75.4 0.0 all-gather.5.cloned.1.call-start
  75.5 34.3 %all_to_all.59 = bf16[8,160,512]{2,1,0:T(8,128)(2,1)} all-to-all(bf16[8,160,512]{2,1,0:T(8,128)(2,1)S(1)} %bitcast.63), channel_id=1, replica_groups=mesh['ep'=8,'tp'=4] {'ep'}, dimensions={0} | all-to-all | bytes 2621440 | tf_op jit(solution)/shard_map/all_to_all | solution.py:57
  109.8 0.0 all-gather.5.cloned.1.call-update
  109.8 0.0 reduce-scatter.2.cloned.1.call-start
  109.9 0.1 all_to_all.52
  110.0 9.6 %all_to_all.60 = f32[8,160,1]{1,2,0:T(1,128)S(1)} all-to-all(f32[8,160,1]{1,2,0:T(1,128)S(1)} %all_to_all.52), channel_id=1, replica_groups=mesh['ep'=8,'tp'=4] {'ep'}, dimensions={0} | all-to-all | bytes 10240 | tf_op jit(solution)/shard_map/all_to_all | solution.py:63
  119.6 0.1 mul.64
  119.6 0.0 copy-done.3
  119.7 5.2 %fusion.6 = f32[1280,256]{1,0:T(8,128)} fusion(bf16[1280,2048]{1,0:T(8,128)(2,1)} %all-gather.3.cloned.1.call-done, bf16[1,2048,256]{2,1,0:T(8,128)(2,1)S(1)} %copy-done.3), kind=kOutput, calls=%fused_computation.27 | convolution fusion | flops 1342177280 | bytes 7602176 | tf_op jit(solution)/shard_map/dot_general | solution.py:74
  124.9 2.6 fusion.12
  127.5 33.1 %all-gather.5.cloned.1.call-done = bf16[1280,2048]{1,0:T(8,128)(2,1)} async-done(((bf16[1280,512]{1,0:T(8,128)(2,1)}), bf16[1280,2048]{1,0:T(8,128)(2,1)}) %all-gather.5.cloned.1.call-update) | async-done | bytes 5242896 | tf_op jit(solution)/shard_map/all_gather | solution.py:61
  160.6 6.5 %select_convert_fusion = (bf16[1280,256]{1,0:T(8,128)(2,1)S(1)}, bf16[1280,256]{1,0:T(8,128)(2,1)S(1)}, bf16[1280,256]{1,0:T(8,128)(2,1)}) fusion(f32[1280,256]{1,0:T(8,128)} %fusion.6, f32[1280,256]{1,0:T(8,128)} %fusion.12, bf16[1,256,2048]{2,1,0:T(8,128)(2,1)S(1)} %copy-done.9, bf16[1280,2048]{1,0:T(8,128)(2,1)} %all-gather.5.cloned.1.call-done, ...), kind=kOutput, calls=%fused_computation.20 | convolution fusion | flops 1357905920 | bytes 10884096 | tf_op jit(solution)/shard_map/rd,fd->rf/dot_general | solution.py:75
  167.1 1.6 fusion.10
  168.7 3.9 %add_convert_fusion = bf16[1280,2048]{1,0:T(8,128)(2,1)} fusion(f32[1280,2048]{1,0:T(8,128)S(1)} %fusion.10, bf16[1280,256]{1,0:T(8,128)(2,1)S(1)} %get-tuple-element.17, bf16[1,2048,256]{2,1,0:T(8,128)(2,1)S(1)} %copy-done.3), kind=kOutput, calls=%fused_computation.11 | convolution fusion | flops 1347420160 | bytes 17432576 | tf_op jit(solution)/shard_map/rf,df->rd/dot_general | solution.py:85
  172.6 0.0 reduce-scatter.2.cloned.1.call-update
  172.6 1.1 copy-done.10
  173.7 4.2 %fusion.1 = f32[1280]{0:T(1024)S(1)} fusion(bf16[1280,2048]{1,0:T(8,128)(2,1)} %all-gather.5.cloned.1.call-done, bf16[1280,256]{1,0:T(8,128)(2,1)S(1)} %copy-done.10, bf16[1,256,2048]{2,1,0:T(8,128)(2,1)S(1)} %copy-done.9), kind=kOutput, calls=%fused_computation.10 | convolution fusion | flops 1355283200 | bytes 6951936 | tf_op jit(solution)/shard_map/dot_general | solution.py:89
  177.8 0.1 all_to_all.49
  177.9 5.3 %psum.7 = f32[8,160,1]{1,0,2:T(8,128)S(1)} all-reduce(f32[8,160,1]{1,0,2:T(8,128)S(1)} %all_to_all.49), channel_id=1, replica_groups=mesh['ep'=8,'tp'=4] {'tp'}, use_global_device_ids=true, to_apply=%region_8.9 | all-reduce | flops 1280 | bytes 10240 | tf_op jit(solution)/shard_map/psum | solution.py:95
  183.3 8.6 %all_to_all.61 = f32[8,160,1]{1,2,0:T(1,128)S(1)} all-to-all(f32[8,160,1]{1,2,0:T(1,128)S(1)} %copy.22), channel_id=1, replica_groups=mesh['ep'=8,'tp'=4] {'ep'}, dimensions={0} | all-to-all | bytes 10240 | tf_op jit(solution)/shard_map/all_to_all | solution.py:99
  191.9 31.5 %reduce-scatter.2.cloned.1.call-done = bf16[1280,512]{1,0:T(8,128)(2,1)} async-done(((bf16[1280,2048]{1,0:T(8,128)(2,1)}), bf16[1280,512]{1,0:T(8,128)(2,1)}) %reduce-scatter.2.cloned.1.call-update) | async-done | bytes 1310736 | tf_op jit(solution)/shard_map/reduce_scatter | solution.py:94
  223.3 5.5 %all-to-all-start.3 = ((bf16[8,160,512]{2,1,0:T(8,128)(2,1)}), bf16[8,160,512]{2,1,0:T(8,128)(2,1)S(1)}, u32[]{:S(2)}, u32[]{:S(2)}) async-start(bf16[8,160,512]{2,1,0:T(8,128)(2,1)} %bitcast.67), calls=%async_computation.4 | async-start | bytes 2621440 | tf_op jit(solution)/shard_map/all_to_all | solution.py:96
  228.9 0.0 slice-start.1
  228.9 5.8 %convolution_bitcast_fusion = f32[1,256,2048]{2,1,0:T(8,128)} fusion(bf16[1280,256]{1,0:T(8,128)(2,1)} %get-tuple-element.19, bf16[1280,2048]{1,0:T(8,128)(2,1)} %all-gather.5.cloned.1.call-done, f32[1280]{0:T(1024)S(1)} %mul.64), kind=kOutput, calls=%fused_computation.13 | convolution fusion | flops 1350041600 | bytes 8000512 | tf_op jit(solution)/shard_map/rf,rd->fd/dot_general | solution.py:83
  234.6 0.0 copy-done.7
  234.6 0.0 slice-done.1
  234.7 3.0 %convolution_bitcast_fusion.1 = f32[1,2048,256]{2,1,0:T(8,128)} fusion(bf16[1280,2048]{1,0:T(8,128)(2,1)S(1)} %bitcast.74, bf16[1280,256]{1,0:T(8,128)(2,1)S(1)} %copy-done.7), kind=kOutput, calls=%fused_computation.14 | convolution fusion | flops 1342177280 | bytes 7995392 | tf_op jit(solution)/shard_map/rd,rf->df/dot_general | solution.py:81
  237.7 0.0 copy-done.5
  237.7 3.0 %convolution_bitcast_fusion.2 = f32[1,2048,256]{2,1,0:T(8,128)} fusion(bf16[1280,2048]{1,0:T(8,128)(2,1)S(1)} %bitcast.74, bf16[1280,256]{1,0:T(8,128)(2,1)S(1)} %copy-done.5), kind=kOutput, calls=%fused_computation.15 | convolution fusion | flops 1342177280 | bytes 7995392 | tf_op jit(solution)/shard_map/rd,rf->df/dot_general | solution.py:78
  240.7 0.1 all_to_all.51
  240.8 6.1 %gather_fusion.4 = f32[1024]{0:T(1024)S(1)} fusion(f32[1280]{0:T(1024)S(1)} %all_to_all.51, s32[1024]{0:T(1024)S(1)} %broadcast_clamp_fusion), kind=kCustom, calls=%fused_computation.4 | custom fusion | bytes 12288 | tf_op jit(solution)/shard_map/gather | solution.py:102
  246.9 0.1 reshape.81
  247.1 0.7 copy.23
  247.8 9.9 %all-to-all-done.3 = bf16[8,160,512]{2,1,0:T(8,128)(2,1)S(1)} async-done(((bf16[8,160,512]{2,1,0:T(8,128)(2,1)}), bf16[8,160,512]{2,1,0:T(8,128)(2,1)S(1)}, u32[]{:S(2)}, u32[]{:S(2)}) %all-to-all-start.3) | async-done | bytes 1310752 | tf_op jit(solution)/shard_map/all_to_all | solution.py:96
  257.7 4.0 %gather_fusion.3 = bf16[1024,512]{1,0:T(8,128)(2,1)S(1)} fusion(bf16[1280,512]{1,0:T(8,128)(2,1)S(1)} %bitcast.62, s32[1024]{0:T(1024)S(1)} %broadcast_clamp_fusion), kind=kCustom, calls=%fused_computation.3 | custom fusion | bytes 2101248 | tf_op jit(solution)/shard_map/gather | solution.py:100
  261.7 0.3 reshape.80
  262.0 2.1 reduce_sum.34
  (28 shorter events, 0.2 us)
Async XLA Ops:
  7.2 117.7 %copy-start = (bf16[1,2048,256]{2,1,0:T(8,128)(2,1)S(1)}, bf16[1,2048,256]{2,1,0:T(8,128)(2,1)}, u32[]{:S(2)}) copy-start(bf16[1,2048,256]{2,1,0:T(8,128)(2,1)} %param.11) | copy-start | bytes 3145732
  7.2 14.7 %copy-start.1 = (bf16[256,2048]{1,0:T(8,128)(2,1)S(1)}, bf16[256,2048]{1,0:T(8,128)(2,1)}, u32[]{:S(2)}) copy-start(bf16[256,2048]{1,0:T(8,128)(2,1)} %param.10) | copy-start | bytes 3145732
  7.2 112.4 %all-gather.3.cloned.1.call-start = ((), (), s32[]{:S(2)}) async-start(), calls=%async_computation.6 | async-start | bytes 6553600 | tf_op jit(solution)/shard_map/all_gather | solution.py:60
  21.9 6.1 %copy-start.2 = (bf16[256,2048]{1,0:T(8,128)(2,1)S(1)}, bf16[256,2048]{1,0:T(8,128)(2,1)}, u32[]{:S(2)}) copy-start(bf16[256,2048]{1,0:T(8,128)(2,1)} %param.7) | copy-start | bytes 3145732
  41.4 78.2 %copy-start.3 = (bf16[1,2048,256]{2,1,0:T(8,128)(2,1)S(1)}, bf16[1,2048,256]{2,1,0:T(8,128)(2,1)}, u32[]{:S(2)}) copy-start(bf16[1,2048,256]{2,1,0:T(8,128)(2,1)} %param.12) | copy-start | bytes 3145732
  75.4 85.1 %all-gather.5.cloned.1.call-start = ((), (), s32[]{:S(2)}) async-start(), calls=%async_computation.7 | async-start | bytes 6553600 | tf_op jit(solution)/shard_map/all_gather | solution.py:61
  109.8 113.5 %reduce-scatter.2.cloned.1.call-start = ((), (), s32[]{:S(2)}) async-start(), calls=%async_computation.8 | async-start | bytes 6553600 | tf_op jit(solution)/shard_map/reduce_scatter | solution.py:94
  119.6 5.2 %copy-start.8 = (bf16[1280,2048]{1,0:T(8,128)(2,1)S(1)}, bf16[1280,2048]{1,0:T(8,128)(2,1)}, u32[]{:S(2)}) copy-start(bf16[1280,2048]{1,0:T(8,128)(2,1)} %all-gather.3.cloned.1.call-done) | copy-start | bytes 15728644
  124.9 35.7 %copy-start.9 = (bf16[1,256,2048]{2,1,0:T(8,128)(2,1)S(1)}, bf16[1,256,2048]{2,1,0:T(8,128)(2,1)}, u32[]{:S(2)}) copy-start(bf16[1,256,2048]{2,1,0:T(8,128)(2,1)} %param.13) | copy-start | bytes 3145732
  167.1 1.6 copy-start.4
  167.1 1.6 copy-start.6
  172.6 1.1 copy-start.10
  223.3 34.3 %all-to-all-start.3 = ((bf16[8,160,512]{2,1,0:T(8,128)(2,1)}), bf16[8,160,512]{2,1,0:T(8,128)(2,1)S(1)}, u32[]{:S(2)}, u32[]{:S(2)}) async-start(bf16[8,160,512]{2,1,0:T(8,128)(2,1)} %bitcast.67), calls=%async_computation.4 | async-start | bytes 2621440 | tf_op jit(solution)/shard_map/all_to_all | solution.py:96
  228.8 5.8 %copy-start.7 = (bf16[1280,256]{1,0:T(8,128)(2,1)S(1)}, bf16[1280,256]{1,0:T(8,128)(2,1)}, u32[]{:S(2)}) copy-start(bf16[1280,256]{1,0:T(8,128)(2,1)} %copy-done.6) | copy-start | bytes 1966084
  228.8 5.8 %slice-start = ((s8[5242880]{0:T(1024)(128)(4,1)}), s8[4194304]{0:T(1024)(128)(4,1)S(1)}, s32[]{:S(2)}) async-start(s8[5242880]{0:T(1024)(128)(4,1)} %bitcast.73), calls=%async_computation.9 | async-start | bytes 8388608
  228.9 5.8 %slice-start.1 = ((s8[5242880]{0:T(1024)(128)(4,1)}), s8[1048576]{0:T(1024)(128)(4,1)S(1)}, s32[]{:S(2)}) async-start(s8[5242880]{0:T(1024)(128)(4,1)} %bitcast.73), calls=%async_computation.10 | async-start | bytes 2097152
  234.7 3.0 %copy-start.5 = (bf16[1280,256]{1,0:T(8,128)(2,1)S(1)}, bf16[1280,256]{1,0:T(8,128)(2,1)}, u32[]{:S(2)}) copy-start(bf16[1280,256]{1,0:T(8,128)(2,1)} %copy-done.4) | copy-start | bytes 1966084
Sparse Core Ops, SparseCore 0:
  75.6 42.9 all-gather.2
  120.1 40.3 all-gather.4
  172.7 50.5 reduce-scatter.1
where the time goes:
time: 275 us; the launch traced here: 271 us
  blocking collectives  91.8 us (33%)
  waiting for transfers between devices  74.6 us (27%)
  local copies, waits for them, and re-layouts  41 us (15%)
  matrix products  35.8 us (13%)
  between operations  14.1 us (5%)
  other arithmetic  7.84 us (3%)
  starting transfers between devices  5.61 us (2%)
    all_to_all x1, blocking collectives, local(): lax.all_to_all(part_grads, 'ep', split_axis=0, concat_axis=0, tiled=True)  34.3 us
    all_to_all x1, blocking collectives, local(): lax.all_to_all(part_rows, 'ep', split_axis=0, concat_axis=0, tiled=True)  34 us
    all_gather x1, waiting for transfers between devices, local(): lax.all_gather(part_grads, 'tp', axis=1, tiled=True)  33.1 us
    reduce_scatter x1, waiting for transfers between devices, local(): lax.psum_scatter(all_rows, 'tp', scatter_dimension=1, tiled=True)  31.5 us
    all_to_all x1, waiting for transfers between devices, local(): lax.all_to_all(row_sum.astype(jnp.bfloat16), 'ep', split_axis=0, concat_a...  9.94 us
    all_to_all x1, blocking collectives, local(): lax.all_to_all(send_weights, 'ep', split_axis=0, concat_axis=0, tiled=True)  9.55 us
    all_to_all x1, blocking collectives, local(): lax.all_to_all(product_sum, 'ep', split_axis=0, concat_axis=0, tiled=True)  8.59 us
    dot_general x1, matrix products, local(): jnp.einsum('rd,fd->rf', scaled, w_down[0], preferred_element_type=jnp.flo...  6.5 us
  transfers between devices with their start and end apart: 4, of which 3 were waited for; matrix products, arithmetic and copies ran while one was open for 11% of the time, Pallas kernels for 0%

commit v1 on v0

v1 whole, which is shorter than its diff:
```python
import jax
import jax.numpy as jnp
from jax import lax
from jax.experimental import pallas as pl
from jax.experimental.pallas import tpu as pltpu
from jax.sharding import PartitionSpec as P

clamp_limit = 7.0
sigmoid_slope = 1.702
MESH = pl.DeviceIdType.MESH


def partners():
    ep_count = lax.axis_size("ep")
    tp_count = lax.axis_size("tp")
    here = lax.axis_index("ep")
    part = lax.axis_index("tp")
    beside = part + 1 - 2 * (part % 2)
    across = (part + tp_count // 2) % tp_count
    return ep_count, here, part, beside, across


def greet(ep_count, here, part, beside, across):
    barrier = pltpu.get_barrier_semaphore()
    pl.semaphore_signal(barrier, inc=1, device_id=(here, beside), device_id_type=MESH)
    pl.semaphore_signal(barrier, inc=1, device_id=(here, across), device_id_type=MESH)

    def call(j, carry):
        peer = (here + j) % ep_count
        pl.semaphore_signal(barrier, inc=1, device_id=(peer, part), device_id_type=MESH)
        return carry

    lax.fori_loop(1, ep_count, call, 0)
    pl.semaphore_wait(barrier, ep_count + 1)


def remote(src, dst, sent, got, device):
    return pltpu.make_async_remote_copy(
        src_ref=src, dst_ref=dst, send_sem=sent, recv_sem=got, device_id=device, device_id_type=MESH
    )


def dispatch_kernel(
    send_ref, weight_ref, rows_ref, weights_out, s1, r1, s2, r2, s3, r3, s4, r4, sw, rw, own_sem
):
    ep_count, here, part, beside, across = partners()
    width = send_ref.shape[3]

    def block(source, owner):
        columns = pl.ds(pl.multiple_of(owner * width, width), width)
        return rows_ref.at[:, source, :, columns]

    greet(ep_count, here, part, beside, across)

    def first(j):
        peer = (here + j) % ep_count
        return remote(send_ref.at[:, peer], block(here, part), s1.at[j], r1.at[j], (peer, part))

    def first_weight(j):
        peer = (here + j) % ep_count
        return remote(
            weight_ref.at[peer], weights_out.at[here], sw.at[j], rw.at[j], (peer, part)
        )

    def near(j):
        source = (here + ep_count - j) % ep_count
        return remote(block(source, part), block(source, part), s2.at[j], r2.at[j], (here, beside))

    def far(j):
        source = (here + ep_count - j) % ep_count
        return remote(block(source, part), block(source, part), s3.at[j], r3.at[j], (here, across))

    def onward(j):
        source = (here + ep_count - j) % ep_count
        return remote(
            block(source, across), block(source, across), s4.at[j], r4.at[j], (here, beside)
        )

    own = pltpu.make_async_copy(send_ref.at[:, here], block(here, part), own_sem.at[0])
    own_weight = pltpu.make_async_copy(weight_ref.at[here], weights_out.at[here], own_sem.at[1])
    own.start()
    own_weight.start()

    def launch(j, carry):
        first_weight(j).start()
        first(j).start()
        return carry

    lax.fori_loop(1, ep_count, launch, 0)
    own.wait()
    far(0).start()
    near(0).start()

    def pass_on(j, carry):
        @pl.when(j < ep_count)
        def _():
            first(j).wait_recv()
            far(j).start()
            near(j).start()

        @pl.when(j >= 2)
        def _():
            far(j - 2).wait_recv()
            onward(j - 2).start()

        return carry

    lax.fori_loop(1, ep_count + 2, pass_on, 0)
    own_weight.wait()

    def finish(j, carry):
        near(j).wait()
        onward(j).wait()
        far(j).wait_send()

        @pl.when(j >= 1)
        def _():
            first(j).wait_send()
            first_weight(j).wait()

        return carry

    lax.fori_loop(0, ep_count, finish, 0)


def dispatch(send, weights, model_width):
    _, ep_count, capacity, width = send.shape
    sems = [pltpu.SemaphoreType.DMA((ep_count,)) for _ in range(10)]
    return pl.pallas_call(
        dispatch_kernel,
        out_shape=(
            jax.ShapeDtypeStruct((2, ep_count, capacity, model_width), jnp.bfloat16),
            jax.ShapeDtypeStruct(weights.shape, jnp.float32),
        ),
        in_specs=[pl.BlockSpec(memory_space=pltpu.VMEM)] * 2,
        out_specs=(pl.BlockSpec(memory_space=pl.ANY), pl.BlockSpec(memory_space=pltpu.VMEM)),
        scratch_shapes=sems + [pltpu.SemaphoreType.DMA((2,))],
        compiler_params=pltpu.CompilerParams(collective_id=0, has_side_effects=True),
    )(send, weights)


def combine_kernel(
    rows_ref, product_ref, back_ref, back_product, near_buf, far_send, far_buf, last_send,
    product_near, product_sum, product_far, product_send,
    s1, r1, s2, r2, s3, r3, sw, rw, small_send, small_recv,
):
    ep_count, here, part, beside, across = partners()
    width = back_ref.shape[2]
    beside_far = (beside + lax.axis_size("tp") // 2) % lax.axis_size("tp")

    def columns(owner):
        return pl.ds(pl.multiple_of(owner * width, width), width)

    greet(ep_count, here, part, beside, across)

    def near(which, j):
        target = (here + j) % ep_count
        owner = beside_far if which == 0 else beside
        return remote(
            rows_ref.at[target, :, columns(owner)], near_buf.at[which, j],
            s1.at[which, j], r1.at[which, j], (here, beside),
        )

    def far(j):
        return remote(far_send.at[j], far_buf.at[j], s2.at[j], r2.at[j], (here, across))

    def last(j):
        peer = (here + j) % ep_count
        return remote(last_send.at[j], back_ref.at[here], s3.at[j], r3.at[j], (peer, part))

    def last_product(j):
        peer = (here + j) % ep_count
        return remote(
            product_send.at[peer], back_product.at[here], sw.at[j], rw.at[j], (peer, part)
        )

    small_near = remote(product_ref, product_near, small_send.at[0], small_recv.at[0], (here, beside))
    small_far = remote(product_sum, product_far, small_send.at[1], small_recv.at[1], (here, across))
    small_near.start()

    def launch(j, carry):
        near(0, j).start()
        near(1, j).start()
        return carry

    lax.fori_loop(0, ep_count, launch, 0)
    small_near.wait_recv()
    product_sum[...] = product_ref[...] + product_near[...]
    small_far.start()

    def middle(j, carry):
        near(0, j).wait_recv()
        target = (here + j) % ep_count
        mine = rows_ref[target, :, columns(across)].astype(jnp.float32)
        far_send[j] = (mine + near_buf[0, j].astype(jnp.float32)).astype(jnp.bfloat16)
        far(j).start()
        return carry

    lax.fori_loop(0, ep_count, middle, 0)
    small_far.wait_recv()
    product_send[...] = product_sum[...] + product_far[...]

    def total(j):
        near(1, j).wait_recv()
        far(j).wait_recv()
        target = (here + j) % ep_count
        mine = rows_ref[target, :, columns(part)].astype(jnp.float32)
        added = mine + near_buf[1, j].astype(jnp.float32) + far_buf[j].astype(jnp.float32)
        return added.astype(jnp.bfloat16)

    def end(j, carry):
        last_send[j] = total(j)
        last(j).start()
        last_product(j).start()
        return carry

    back_ref[here] = total(0)
    back_product[here] = product_send[here]
    lax.fori_loop(1, ep_count, end, 0)

    small_near.wait_send()
    small_far.wait_send()

    def finish(j, carry):
        near(0, j).wait_send()
        near(1, j).wait_send()
        far(j).wait_send()

        @pl.when(j >= 1)
        def _():
            last(j).wait()
            last_product(j).wait()

        return carry

    lax.fori_loop(0, ep_count, finish, 0)


def combine(rows, products, width):
    ep_count, capacity, _ = rows.shape
    one = (ep_count, capacity, width)
    small = pltpu.VMEM(products.shape, jnp.float32)
    dma = pltpu.SemaphoreType.DMA
    return pl.pallas_call(
        combine_kernel,
        out_shape=(
            jax.ShapeDtypeStruct(one, jnp.bfloat16),
            jax.ShapeDtypeStruct(products.shape, jnp.float32),
        ),
        in_specs=[pl.BlockSpec(memory_space=pltpu.VMEM)] * 2,
        out_specs=(pl.BlockSpec(memory_space=pltpu.VMEM),) * 2,
        scratch_shapes=[
            pltpu.VMEM((2,) + one, jnp.bfloat16),
            pltpu.VMEM(one, jnp.bfloat16),
            pltpu.VMEM(one, jnp.bfloat16),
            pltpu.VMEM(one, jnp.bfloat16),
            small, small, small, small,
            dma((2, ep_count)), dma((2, ep_count)),
            dma((ep_count,)), dma((ep_count,)), dma((ep_count,)), dma((ep_count,)),
            dma((ep_count,)), dma((ep_count,)), dma((2,)), dma((2,)),
        ],
        compiler_params=pltpu.CompilerParams(
            collective_id=1, has_side_effects=True, vmem_limit_bytes=48 * 1024 * 1024
        ),
    )(rows, products)


def local(tokens, routes, gate_weights, out_grad, w_gate, w_up, w_down):
    f32, bf16 = jnp.float32, jnp.bfloat16
    ep_count = lax.axis_size("ep")
    tp_count = lax.axis_size("tp")
    part = lax.axis_index("tp")
    token_count, model_width = tokens.shape
    top_count = routes.shape[1]
    experts = ep_count * w_gate.shape[0]
    capacity = token_count * top_count * 5 // (4 * experts)
    width = model_width // tp_count

    match = routes[:, :, None] == jnp.arange(experts, dtype=jnp.int32)[None, None, :]
    named = jnp.any(match, axis=1)
    before = jnp.arange(token_count)[:, None] > jnp.arange(token_count)[None, :]
    rank = jnp.dot(before.astype(bf16), named.astype(bf16), preferred_element_type=f32)
    rank = jnp.where(named, rank.astype(jnp.int32), -1)
    pick = rank.T[:, None, :] == jnp.arange(capacity, dtype=jnp.int32)[None, :, None]
    pick_flat = pick.reshape(experts * capacity, token_count).astype(bf16)
    weight_of = jnp.sum(jnp.where(match, gate_weights[:, :, None], 0.0), axis=1)
    send_weights = jnp.sum(jnp.where(pick, weight_of.T[:, None, :], 0.0), axis=2)
    own = jnp.stack(
        [lax.dynamic_slice_in_dim(a, part * width, width, 1) for a in (tokens, out_grad)]
    )
    send = jnp.einsum("rt,atw->arw", pick_flat, own, preferred_element_type=f32).astype(bf16)
    send = send.reshape(2, experts, capacity, width)

    both, weights = dispatch(send, send_weights[:, None, :], model_width)
    row_count = ep_count * capacity
    x_rows = both[0].reshape(row_count, model_width)
    dy_rows = both[1].reshape(row_count, model_width)
    slot_weights = weights.reshape(row_count, 1)

    gate_pre = jnp.dot(x_rows, w_gate[0], preferred_element_type=f32)
    up_pre = jnp.dot(x_rows, w_up[0], preferred_element_type=f32)
    plain_grad = jnp.einsum("rd,fd->rf", dy_rows, w_down[0], preferred_element_type=f32)
    glu = jnp.minimum(gate_pre, clamp_limit)
    linear = jnp.clip(up_pre, -clamp_limit, clamp_limit)
    sigma = jax.nn.sigmoid(sigmoid_slope * glu)
    active = glu * sigma
    hidden = active * (linear + 1.0)
    product = jnp.sum(hidden * plain_grad, axis=1)
    hidden_grad = plain_grad * slot_weights
    slope_term = sigma + sigmoid_slope * active * (1.0 - sigma)
    gate_pre_grad = jnp.where(
        gate_pre < clamp_limit, hidden_grad * (linear + 1.0) * slope_term, 0.0
    ).astype(bf16)
    up_pre_grad = jnp.where(jnp.abs(up_pre) < clamp_limit, hidden_grad * active, 0.0).astype(bf16)
    hidden = (hidden * slot_weights).astype(bf16)

    row_term = jnp.einsum("rf,df->rd", gate_pre_grad, w_gate[0], preferred_element_type=f32)
    row_term = row_term + jnp.einsum(
        "rf,df->rd", up_pre_grad, w_up[0], preferred_element_type=f32
    )
    row_term = row_term.astype(bf16).reshape(ep_count, capacity, model_width)
    back_rows, back_products = combine(
        row_term, product.reshape(ep_count, 1, capacity), width
    )
    gate_grads = jnp.einsum("rd,rf->df", x_rows, gate_pre_grad, preferred_element_type=f32)
    up_grads = jnp.einsum("rd,rf->df", x_rows, up_pre_grad, preferred_element_type=f32)
    down_grads = jnp.einsum("rf,rd->fd", hidden, dy_rows, preferred_element_type=f32)
    token_grad = jnp.einsum(
        "rt,rw->tw", pick_flat, back_rows.reshape(row_count, width), preferred_element_type=f32
    ).astype(bf16)
    found = jnp.sum(jnp.where(pick, back_products.reshape(experts, capacity, 1), 0.0), axis=1)
    gate_grad = jnp.sum(jnp.where(match, found.T[:, None, :], 0.0), axis=2)
    return (token_grad, gate_grad, gate_grads[None], up_grads[None], down_grads[None])


def solution(mesh):
    return jax.shard_map(
        local,
        mesh=mesh,
        in_specs=(
            P("ep", None),
            P("ep", None),
            P("ep", None),
            P("ep", None),
            P("ep", None, "tp"),
            P("ep", None, "tp"),
            P("ep", "tp", None),
        ),
        out_specs=(
            P("ep", "tp"),
            P("ep", None),
            P("ep", None, "tp"),
            P("ep", None, "tp"),
            P("ep", "tp", None),
        ),
        check_vma=False,
    )
```

time: 275 us -> 201 us (0.73); the launches traced: 271 us -> 200 us
  Pallas kernels: 0 us -> 145 us
  blocking collectives: 91.8 us -> 0 us
  waiting for transfers between devices: 74.6 us -> 0 us
  local copies, waits for them, and re-layouts: 41 us -> 17 us
  between operations: 14.1 us -> 0.85 us
  starting transfers between devices: 5.61 us -> 0 us
  other arithmetic: 7.84 us -> 3.02 us
    pallas_call x0 -> x2, Pallas kernels: none -> 145 us  [the longest x1 81.7 us: dispatch(): pl.pallas_call(dispatch_kernel, out_shape=(jax.ShapeDtypeStruct((2, ep_co...]
    all_to_all x4 -> x0, blocking collectives: 86.5 us -> none  [the longest x1 34.3 us: local(): lax.all_to_all(part_grads, 'ep', split_axis=0, concat_axis=0, tiled=True)]
    all_gather x2 -> x0, waiting for transfers between devices: 33.1 us -> none  [the longest x1 33.1 us: local(): lax.all_gather(part_grads, 'tp', axis=1, tiled=True)]
    reduce_scatter x1 -> x0, waiting for transfers between devices: 31.5 us -> none  [local(): lax.psum_scatter(all_rows, 'tp', scatter_dimension=1, tiled=True)]
    gather x5 -> x0, local copies, waits for them, and re-layouts: 27.3 us -> none  [the longest x1 6.15 us: local(): gate_grad = back_products[target].reshape(token_count, top_count)]
    slice x1, local copies, waits for them, and re-layouts: 0.28 us -> 10.3 us  [local(): dy_rows = both[1].reshape(row_count, model_width)]
    all_to_all x1 -> x0, waiting for transfers between devices: 9.94 us -> none  [local(): lax.all_to_all(row_sum.astype(jnp.bfloat16), 'ep', split_axis=0, concat_a...]
    scatter x2 -> x0, local copies, waits for them, and re-layouts: 8.63 us -> none  [the longest x1 4.32 us: local(): jnp.zeros((experts_all * capacity,), jnp.int32).at[target].set(pair_index)]
  transfers between devices with their start and end apart: 4 -> 0, of which waited for: 3 -> 0; matrix products, arithmetic and copies ran while one was open for 11% -> 0% of each run, Pallas kernels for 0% -> 0%
where the time goes in v1:
time: 201 us; the launch traced here: 200 us
  Pallas kernels  145 us (72%)
  matrix products  33.9 us (17%)
  local copies, waits for them, and re-layouts  17 us (8%)
  other arithmetic  3.02 us (2%)
    pallas_call x1, Pallas kernels, dispatch(): pl.pallas_call(dispatch_kernel, out_shape=(jax.ShapeDtypeStruct((2, ep_co...  81.7 us
    pallas_call x1, Pallas kernels, combine(): pl.pallas_call(combine_kernel, out_shape=(jax.ShapeDtypeStruct(one, jnp.b...  63.6 us
    slice x1, local copies, waits for them, and re-layouts, local(): dy_rows = both[1].reshape(row_count, model_width)  10.3 us
    dot_general x1, matrix products, local(): jnp.einsum('rd,rf->df', x_rows, up_pre_grad, preferred_element_type=f32)  5.71 us
    dot_general x1, matrix products, local(): jnp.einsum('rd,rf->df', x_rows, gate_pre_grad, preferred_element_type=f32)  5.71 us
    convert_element_type x1, local copies, waits for them, and re-layouts, local(): jnp.einsum('rt,atw->arw', pick_flat, own, preferred_element_type=f32)  4.44 us
    dot_general x1, matrix products, local(): up_pre = jnp.dot(x_rows, w_up[0], preferred_element_type=f32)  4.19 us

profile of v1, /device:TPU:11, one launch (start us, length us, event | category | flops | bytes accessed | tf_op | source)
XLA Modules:
  0.0 200.1 jit_solution(438271991620336590)
XLA Ops:
  0.6 0.0 copy-start
  0.7 0.8 fusion.22
  1.4 0.2 fusion.6
  1.6 0.7 select_reduce_fusion.3
  2.3 0.3 select_reduce_fusion.1
  2.7 0.6 broadcast_in_dim.81.weight_ref
  3.3 0.1 eq.45
  3.4 0.2 bitcast_compare_fusion
  3.6 1.1 constant_dynamic-slice_fusion
  4.7 0.1 copy.24
  4.9 0.1 copy.23
  5.0 2.4 %fusion = bf16[2,1280,512]{1,2,0:T(8,128)(2,1)} fusion(pred[1280,256]{1,0:T(32,128)(4,1)S(1)} %bitcast_compare_fusion, bf16[1,256,512]{1,2,0:T(8,128)(2,1)S(1)} %bitcast.65, bf16[1,256,512]{1,2,0:T(8,128)(2,1)S(1)} %bitcast.66), kind=kOutput, calls=%fused_computation.2 | convolution fusion | flops 672661504 | bytes 3473408 | tf_op jit(solution)/shard_map/rt,atw->arw/dot_general | solution.py:291
  7.4 4.4 %copy.25 = bf16[2,1280,512]{2,1,0:T(8,128)(2,1)} copy(bf16[2,1280,512]{1,2,0:T(8,128)(2,1)} %fusion) | data formatting | bytes 5242880 | tf_op jit(solution)/shard_map/convert_element_type | solution.py:291
  11.8 81.7 %shard_map.110 = (bf16[2,8,160,2048]{3,2,1,0:T(8,128)(2,1)}, f32[8,1,160]{2,1,0:T(1,128)}) custom-call(bf16[2,8,160,512]{3,2,1,0:T(8,128)(2,1)} %bitcast.56, f32[8,1,160]{2,1,0:T(1,128)} %broadcast_in_dim.81.weight_ref), custom_call_target="tpu_custom_call" | custom-call | tf_op jit(solution)/shard_map/pallas_call | solution.py:129
  93.5 0.0 copy-start.8
  93.5 0.0 copy-start.5
  93.5 10.3 %fusion.27 = (bf16[1,8,160,2048]{3,2,1,0:T(8,128)(2,1)}, bf16[1,8,160,2048]{3,2,1,0:T(8,128)(2,1)}) fusion(bf16[2,8,160,2048]{3,2,1,0:T(8,128)(2,1)} %get-tuple-element.9), kind=kLoop, calls=%fused_computation.51 | loop fusion | bytes 20971520 | tf_op jit(solution)/shard_map/slice | solution.py:297
  103.8 0.0 copy-done.8
  103.8 0.1 mul.48
  103.9 0.0 copy-done.5
  103.9 0.0 copy-start.1
  103.9 0.0 slice-start
  103.9 4.2 %fusion.8 = f32[1280,256]{0,1:T(8,128)S(1)} fusion(bf16[1280,2048]{1,0:T(8,128)(2,1)} %bitcast.57, bf16[1,2048,256]{2,1,0:T(8,128)(2,1)S(1)} %copy-done.5), kind=kOutput, calls=%fused_computation.26 | convolution fusion | flops 1342177280 | bytes 7602176 | tf_op jit(solution)/shard_map/dot_general | solution.py:301
  108.1 0.0 copy-done
  108.1 0.0 copy-done.1
  108.1 0.0 slice-start.1
  108.2 0.0 copy-start.9
  108.2 1.7 fusion.14
  109.9 0.0 slice-done
  109.9 0.0 slice-done.1
  109.9 0.1 copy-done.9
  110.0 0.0 copy-start.2
  110.0 3.4 %multiply_reduce_fusion = (f32[1280]{0:T(1024)S(1)}, bf16[1280,256]{0,1:T(8,128)(2,1)}, f32[1280,256]{0,1:T(8,128)}) fusion(f32[1280,256]{0,1:T(8,128)S(1)} %fusion.8, f32[1280,256]{0,1:T(8,128)S(1)} %fusion.14, f32[1280]{0:T(1024)S(1)} %mul.48, bf16[1280,2048]{1,0:T(8,128)(2,1)S(1)} %bitcast.63, bf16[1,256,2048]{2,1,0:T(8,128)(2,1)S(1)} %copy-done.9), kind=kOutput, calls=%fused_computation.9 | convolution fusion | flops 1347746560 | bytes 10889216 | tf_op jit(solution)/shard_map/rd,fd->rf/dot_general | solution.py:302
  113.4 0.0 copy-done.2
  113.4 3.2 %convolution_bitcast_fusion = f32[1,256,2048]{2,1,0:T(8,128)} fusion(bf16[1280,2048]{1,0:T(8,128)(2,1)S(1)} %bitcast.64, f32[1280]{0:T(1024)S(1)} %mul.48, f32[1280,256]{0,1:T(8,128)S(1)} %fusion.8, f32[1280,256]{0,1:T(8,128)S(1)} %fusion.14), kind=kOutput, calls=%fused_computation.3 | convolution fusion | flops 1345781760 | bytes 9966592 | tf_op jit(solution)/shard_map/rf,rd->fd/dot_general | solution.py:327
  116.5 0.1 reshape.34.product_ref
  116.6 0.0 copy-start.3
  116.6 0.0 copy-start.4
  116.6 5.7 %convolution_bitcast_fusion.1 = f32[1,2048,256]{2,1,0:T(8,128)} fusion(bf16[1280,2048]{1,0:T(8,128)(2,1)} %bitcast.58, bf16[1280,256]{0,1:T(8,128)(2,1)} %get-tuple-element.16), kind=kOutput, calls=%fused_computation.4 | convolution fusion | flops 1342177280 | bytes 7995392 | tf_op jit(solution)/shard_map/rd,rf->df/dot_general | solution.py:326
  122.3 0.0 copy-done.3
  122.3 0.0 copy-done.4
  122.3 5.7 %convolution_bitcast_fusion.2 = f32[1,2048,256]{2,1,0:T(8,128)} fusion(bf16[1280,2048]{1,0:T(8,128)(2,1)} %bitcast.59, f32[1280,256]{0,1:T(8,128)S(1)} %copy-done.3, f32[1280,256]{0,1:T(8,128)S(1)} %copy-done.4, f32[1280,256]{0,1:T(8,128)S(1)} %fusion.8, f32[1280]{0:T(1024)S(1)} %mul.48), kind=kOutput, calls=%fused_computation.5 | convolution fusion | flops 1348075520 | bytes 11277312 | tf_op jit(solution)/shard_map/rd,rf->df/dot_general | solution.py:325
  128.0 0.0 copy-start.6
  128.0 2.4 %fusion.12 = f32[1280,2048]{1,0:T(8,128)S(1)} fusion(bf16[1,2048,256]{2,1,0:T(8,128)(2,1)S(1)} %copy-done, f32[1280,256]{0,1:T(8,128)S(1)} %copy-done.3, f32[1280,256]{0,1:T(8,128)S(1)} %copy-done.4, f32[1280,256]{0,1:T(8,128)S(1)} %fusion.8, f32[1280]{0:T(1024)S(1)} %mul.48), kind=kOutput, calls=%fused_computation.30 | convolution fusion | flops 1348075520 | bytes 15471616 | tf_op jit(solution)/shard_map/rf,df->rd/dot_general | solution.py:317
  130.4 0.0 copy-done.6
  130.4 3.9 %add_convert_fusion = bf16[1280,2048]{1,0:T(8,128)(2,1)} fusion(f32[1280,2048]{1,0:T(8,128)S(1)} %fusion.12, bf16[1280,256]{0,1:T(8,128)(2,1)S(1)} %copy-done.6, bf16[1,2048,256]{2,1,0:T(8,128)(2,1)S(1)} %copy-done.5), kind=kOutput, calls=%fused_computation | convolution fusion | flops 1347420160 | bytes 17432576 | tf_op jit(solution)/shard_map/rf,df->rd/dot_general | solution.py:318
  134.3 63.6 %shard_map.111 = (bf16[8,160,512]{2,1,0:T(8,128)(2,1)S(1)}, f32[8,1,160]{2,1,0:T(1,128)S(1)}) custom-call(bf16[8,160,2048]{2,1,0:T(8,128)(2,1)} %bitcast.55, f32[8,1,160]{2,1,0:T(1,128)S(1)} %reshape.34.product_ref), custom_call_target="tpu_custom_call" | custom-call | tf_op jit(solution)/shard_map/pallas_call | solution.py:244
  198.0 0.0 copy-start.7
  198.0 1.3 fusion.4
  199.2 0.2 select_reduce_fusion
  199.5 0.0 copy-done.7
  199.5 0.6 select_reduce_fusion.2
  (4 shorter events, 0.0 us)
Async XLA Ops:
  0.6 107.5 %copy-start = (bf16[1,2048,256]{2,1,0:T(8,128)(2,1)S(1)}, bf16[1,2048,256]{2,1,0:T(8,128)(2,1)}, u32[]{:S(2)}) copy-start(bf16[1,2048,256]{2,1,0:T(8,128)(2,1)} %param.11) | copy-start | bytes 3145732
  93.5 10.3 %copy-start.8 = (f32[8,1,160]{2,1,0:T(1,128)S(1)}, f32[8,1,160]{2,1,0:T(1,128)}, u32[]{:S(2)}) copy-start(f32[8,1,160]{2,1,0:T(1,128)} %get-tuple-element.10) | copy-start | bytes 15364
  93.5 10.4 %copy-start.5 = (bf16[1,2048,256]{2,1,0:T(8,128)(2,1)S(1)}, bf16[1,2048,256]{2,1,0:T(8,128)(2,1)}, u32[]{:S(2)}) copy-start(bf16[1,2048,256]{2,1,0:T(8,128)(2,1)} %param.12) | copy-start | bytes 3145732
  103.9 4.2 %copy-start.1 = (bf16[1,8,160,2048]{3,2,1,0:T(8,128)(2,1)S(1)}, bf16[1,8,160,2048]{3,2,1,0:T(8,128)(2,1)}, u32[]{:S(2)}) copy-start(bf16[1,8,160,2048]{3,2,1,0:T(8,128)(2,1)} %get-tuple-element.14) | copy-start | bytes 15728644
  103.9 6.0 %slice-start = ((s8[5242880]{0:T(1024)(128)(4,1)}), s8[4194304]{0:T(1024)(128)(4,1)S(1)}, s32[]{:S(2)}) async-start(s8[5242880]{0:T(1024)(128)(4,1)} %bitcast.61), calls=%async_computation | async-start | bytes 8388608
  108.1 1.7 slice-start.1
  108.2 1.8 copy-start.9
  110.0 3.4 %copy-start.2 = (f32[1280,256]{0,1:T(8,128)}, f32[1280,256]{0,1:T(8,128)S(1)}, u32[]{:S(2)}) copy-start(f32[1280,256]{0,1:T(8,128)S(1)} %fusion.14) | copy-start | bytes 3932164
  116.6 5.7 %copy-start.3 = (f32[1280,256]{0,1:T(8,128)S(1)}, f32[1280,256]{0,1:T(8,128)}, u32[]{:S(2)}) copy-start(f32[1280,256]{0,1:T(8,128)} %copy-done.2) | copy-start | bytes 3932164
  116.6 5.7 %copy-start.4 = (f32[1280,256]{0,1:T(8,128)S(1)}, f32[1280,256]{0,1:T(8,128)}, u32[]{:S(2)}) copy-start(f32[1280,256]{0,1:T(8,128)} %get-tuple-element.17) | copy-start | bytes 3932164
  128.0 2.4 %copy-start.6 = (bf16[1280,256]{0,1:T(8,128)(2,1)S(1)}, bf16[1280,256]{0,1:T(8,128)(2,1)}, u32[]{:S(2)}) copy-start(bf16[1280,256]{0,1:T(8,128)(2,1)} %get-tuple-element.16) | copy-start | bytes 1966084
  198.0 1.5 copy-start.7

commit v2 on v1

--- a/solution.py
+++ b/solution.py
@@ -41,20 +41,25 @@
 
 
 def dispatch_kernel(
-    send_ref, weight_ref, rows_ref, weights_out, s1, r1, s2, r2, s3, r3, s4, r4, sw, rw, own_sem
+    token_ref, grad_ref, weight_ref, token_rows, grad_rows, weights_out,
+    s1, r1, s2, r2, s3, r3, s4, r4, sw, rw, own_sem,
 ):
     ep_count, here, part, beside, across = partners()
-    width = send_ref.shape[3]
-
-    def block(source, owner):
+    width = token_ref.shape[2]
+    pairs = ((0, token_ref, token_rows), (1, grad_ref, grad_rows))
+
+    def block(rows_ref, source, owner):
         columns = pl.ds(pl.multiple_of(owner * width, width), width)
-        return rows_ref.at[:, source, :, columns]
+        return rows_ref.at[source, :, columns]
 
     greet(ep_count, here, part, beside, across)
 
     def first(j):
         peer = (here + j) % ep_count
-        return remote(send_ref.at[:, peer], block(here, part), s1.at[j], r1.at[j], (peer, part))
+        return [
+            remote(send.at[peer], block(rows, here, part), s1.at[i, j], r1.at[i, j], (peer, part))
+            for i, send, rows in pairs
+        ]
 
     def first_weight(j):
         peer = (here + j) % ep_count
@@ -62,60 +67,73 @@
             weight_ref.at[peer], weights_out.at[here], sw.at[j], rw.at[j], (peer, part)
         )
 
+    def forward(j, owner, sent, got, to):
+        source = (here + ep_count - j) % ep_count
+        return [
+            remote(
+                block(rows, source, owner), block(rows, source, owner),
+                sent.at[i, j], got.at[i, j], (here, to),
+            )
+            for i, _, rows in pairs
+        ]
+
     def near(j):
-        source = (here + ep_count - j) % ep_count
-        return remote(block(source, part), block(source, part), s2.at[j], r2.at[j], (here, beside))
+        return forward(j, part, s2, r2, beside)
 
     def far(j):
-        source = (here + ep_count - j) % ep_count
-        return remote(block(source, part), block(source, part), s3.at[j], r3.at[j], (here, across))
+        return forward(j, part, s3, r3, across)
 
     def onward(j):
-        source = (here + ep_count - j) % ep_count
-        return remote(
-            block(source, across), block(source, across), s4.at[j], r4.at[j], (here, beside)
-        )
-
-    own = pltpu.make_async_copy(send_ref.at[:, here], block(here, part), own_sem.at[0])
-    own_weight = pltpu.make_async_copy(weight_ref.at[here], weights_out.at[here], own_sem.at[1])
-    own.start()
-    own_weight.start()
+        return forward(j, across, s4, r4, beside)
+
+    owns = [
+        pltpu.make_async_copy(send.at[here], block(rows, here, part), own_sem.at[i])
+        for i, send, rows in pairs
+    ]
+    owns.append(pltpu.make_async_copy(weight_ref.at[here], weights_out.at[here], own_sem.at[2]))
+    for copy in owns:
+        copy.start()
 
     def launch(j, carry):
         first_weight(j).start()
-        first(j).start()
+        for copy in first(j):
+            copy.start()
         return carry
 
     lax.fori_loop(1, ep_count, launch, 0)
-    own.wait()
-    far(0).start()
-    near(0).start()
+    for copy in owns:
+        copy.wait()
+    for copy in far(0) + near(0):
+        copy.start()
 
     def pass_on(j, carry):
         @pl.when(j < ep_count)
         def _():
-            first(j).wait_recv()
-            far(j).start()
-            near(j).start()
+            for i in range(2):
+                first(j)[i].wait_recv()
+                far(j)[i].start()
+                near(j)[i].start()
 
         @pl.when(j >= 2)
         def _():
-            far(j - 2).wait_recv()
-            onward(j - 2).start()
+            for i in range(2):
+                far(j - 2)[i].wait_recv()
+                onward(j - 2)[i].start()
 
         return carry
 
     lax.fori_loop(1, ep_count + 2, pass_on, 0)
-    own_weight.wait()
 
     def finish(j, carry):
-        near(j).wait()
-        onward(j).wait()
-        far(j).wait_send()
+        for i in range(2):
+            near(j)[i].wait()
+            onward(j)[i].wait()
+            far(j)[i].wait_send()
 
         @pl.when(j >= 1)
         def _():
-            first(j).wait_send()
+            for copy in first(j):
+                copy.wait_send()
             first_weight(j).wait()
 
         return carry
@@ -123,20 +141,23 @@
     lax.fori_loop(0, ep_count, finish, 0)
 
 
-def dispatch(send, weights, model_width):
-    _, ep_count, capacity, width = send.shape
-    sems = [pltpu.SemaphoreType.DMA((ep_count,)) for _ in range(10)]
+def dispatch(send_tokens, send_grads, weights, model_width):
+    ep_count, capacity, width = send_tokens.shape
+    sems = [pltpu.SemaphoreType.DMA((2, ep_count)) for _ in range(8)]
+    sems += [pltpu.SemaphoreType.DMA((ep_count,)) for _ in range(2)]
+    whole = jax.ShapeDtypeStruct((ep_count, capacity, model_width), jnp.bfloat16)
     return pl.pallas_call(
         dispatch_kernel,
-        out_shape=(
-            jax.ShapeDtypeStruct((2, ep_count, capacity, model_width), jnp.bfloat16),
-            jax.ShapeDtypeStruct(weights.shape, jnp.float32),
-        ),
-        in_specs=[pl.BlockSpec(memory_space=pltpu.VMEM)] * 2,
-        out_specs=(pl.BlockSpec(memory_space=pl.ANY), pl.BlockSpec(memory_space=pltpu.VMEM)),
-        scratch_shapes=sems + [pltpu.SemaphoreType.DMA((2,))],
+        out_shape=(whole, whole, jax.ShapeDtypeStruct(weights.shape, jnp.float32)),
+        in_specs=[pl.BlockSpec(memory_space=pltpu.VMEM)] * 3,
+        out_specs=(
+            pl.BlockSpec(memory_space=pl.ANY),
+            pl.BlockSpec(memory_space=pl.ANY),
+            pl.BlockSpec(memory_space=pltpu.VMEM),
+        ),
+        scratch_shapes=sems + [pltpu.SemaphoreType.DMA((3,))],
         compiler_params=pltpu.CompilerParams(collective_id=0, has_side_effects=True),
-    )(send, weights)
+    )(send_tokens, send_grads, weights)
 
 
 def combine_kernel(
@@ -178,7 +199,8 @@
     small_far = remote(product_sum, product_far, small_send.at[1], small_recv.at[1], (here, across))
     small_near.start()
 
-    def launch(j, carry):
+    def launch(step, carry):
+        j = (step + 1) % ep_count
         near(0, j).start()
         near(1, j).start()
         return carry
@@ -188,7 +210,8 @@
     product_sum[...] = product_ref[...] + product_near[...]
     small_far.start()
 
-    def middle(j, carry):
+    def middle(step, carry):
+        j = (step + 1) % ep_count
         near(0, j).wait_recv()
         target = (here + j) % ep_count
         mine = rows_ref[target, :, columns(across)].astype(jnp.float32)
@@ -214,9 +237,9 @@
         last_product(j).start()
         return carry
 
+    lax.fori_loop(1, ep_count, end, 0)
     back_ref[here] = total(0)
     back_product[here] = product_send[here]
-    lax.fori_loop(1, ep_count, end, 0)
 
     small_near.wait_send()
     small_far.wait_send()
@@ -285,16 +308,16 @@
     pick_flat = pick.reshape(experts * capacity, token_count).astype(bf16)
     weight_of = jnp.sum(jnp.where(match, gate_weights[:, :, None], 0.0), axis=1)
     send_weights = jnp.sum(jnp.where(pick, weight_of.T[:, None, :], 0.0), axis=2)
-    own = jnp.stack(
-        [lax.dynamic_slice_in_dim(a, part * width, width, 1) for a in (tokens, out_grad)]
-    )
-    send = jnp.einsum("rt,atw->arw", pick_flat, own, preferred_element_type=f32).astype(bf16)
-    send = send.reshape(2, experts, capacity, width)
-
-    both, weights = dispatch(send, send_weights[:, None, :], model_width)
+    sends = []
+    for array in (tokens, out_grad):
+        own = lax.dynamic_slice_in_dim(array, part * width, width, 1)
+        picked = jnp.dot(pick_flat, own, preferred_element_type=f32).astype(bf16)
+        sends.append(picked.reshape(experts, capacity, width))
+
+    rows, grads, weights = dispatch(*sends, send_weights[:, None, :], model_width)
     row_count = ep_count * capacity
-    x_rows = both[0].reshape(row_count, model_width)
-    dy_rows = both[1].reshape(row_count, model_width)
+    x_rows = rows.reshape(row_count, model_width)
+    dy_rows = grads.reshape(row_count, model_width)
     slot_weights = weights.reshape(row_count, 1)
 
     gate_pre = jnp.dot(x_rows, w_gate[0], preferred_element_type=f32)

time: 201 us -> 182 us (0.905)
  local copies, waits for them, and re-layouts: 17 us -> 0.95 us
  Pallas kernels: 145 us -> 140 us
  matrix products: 33.9 us -> 36.7 us
    slice x1 -> x0, local copies, waits for them, and re-layouts: 10.3 us -> none  [local(): dy_rows = both[1].reshape(row_count, model_width)]
    convert_element_type x1 -> x0, local copies, waits for them, and re-layouts: 4.44 us -> none  [local(): jnp.einsum('rt,atw->arw', pick_flat, own, preferred_element_type=f32)]
    pallas_call x1, Pallas kernels: 81.7 us -> 78.6 us  [dispatch(): pl.pallas_call(dispatch_kernel, out_shape=(whole, whole, jax.ShapeDtypeSt...]
    dot_general x1 -> x2, matrix products: 2.4 us -> 5.05 us  [local(): picked = jnp.dot(pick_flat, own, preferred_element_type=f32).astype(bf16)]
    pallas_call x1, Pallas kernels: 63.6 us -> 61.1 us  [combine(): pl.pallas_call(combine_kernel, out_shape=(jax.ShapeDtypeStruct(one, jnp.b...]
where the time goes in v2:
time: 182 us
  Pallas kernels  140 us (77%)
  matrix products  36.7 us (20%)
  other arithmetic  3.71 us (2%)
    pallas_call x1, Pallas kernels, dispatch(): pl.pallas_call(dispatch_kernel, out_shape=(whole, whole, jax.ShapeDtypeSt...  78.6 us
    pallas_call x1, Pallas kernels, combine(): pl.pallas_call(combine_kernel, out_shape=(jax.ShapeDtypeStruct(one, jnp.b...  61.1 us
    dot_general x1, matrix products, local(): jnp.einsum('rd,rf->df', x_rows, up_pre_grad, preferred_element_type=f32)  5.71 us
    dot_general x1, matrix products, local(): jnp.einsum('rd,rf->df', x_rows, gate_pre_grad, preferred_element_type=f32)  5.71 us
    dot_general x2, matrix products, local(): picked = jnp.dot(pick_flat, own, preferred_element_type=f32).astype(bf16)  5.05 us
    dot_general x1, matrix products, local(): up_pre = jnp.dot(x_rows, w_up[0], preferred_element_type=f32)  4.24 us
    dot_general x1, matrix products, local(): jnp.einsum('rf,df->rd', up_pre_grad, w_up[0], preferred_element_type=f32)  3.93 us

profile of v2, /device:TPU:11, one launch (start us, length us, event | category | flops | bytes accessed | tf_op | source)
XLA Modules:
  0.0 181.9 jit_solution(12372572740274645260)
XLA Ops:
  0.6 0.0 copy-start
  0.7 0.8 fusion.19
  1.4 0.2 fusion.4
  1.6 0.7 select_reduce_fusion.3
  2.3 0.3 select_reduce_fusion.1
  2.7 0.6 broadcast_in_dim.81.weight_ref
  3.3 0.1 eq.45
  3.4 0.2 bitcast_compare_fusion
  3.6 2.5 %convolution_convert_fusion = bf16[1280,512]{1,0:T(8,128)(2,1)} fusion(pred[1280,256]{1,0:T(32,128)(4,1)S(1)} %bitcast_compare_fusion, bf16[256,2048]{1,0:T(8,128)(2,1)} %param.10, s32[]{:T(128)S(6)} %select_n.33), kind=kOutput, calls=%fused_computation.1 | convolution fusion | flops 336199680 | bytes 1900548 | tf_op jit(solution)/shard_map/dot_general | solution.py:314
  6.2 2.5 %convolution_convert_fusion.1 = bf16[1280,512]{1,0:T(8,128)(2,1)} fusion(pred[1280,256]{1,0:T(32,128)(4,1)S(1)} %bitcast_compare_fusion, bf16[256,2048]{1,0:T(8,128)(2,1)} %param.7, s32[]{:T(128)S(6)} %select_n.33), kind=kOutput, calls=%fused_computation.2 | convolution fusion | flops 336199680 | bytes 1900548 | tf_op jit(solution)/shard_map/dot_general | solution.py:314
  8.7 0.0 copy-start.4
  8.7 78.6 %shard_map.110 = (bf16[8,160,2048]{2,1,0:T(8,128)(2,1)}, bf16[8,160,2048]{2,1,0:T(8,128)(2,1)}, f32[8,1,160]{2,1,0:T(1,128)}) custom-call(bf16[8,160,512]{2,1,0:T(8,128)(2,1)} %bitcast.53, bf16[8,160,512]{2,1,0:T(8,128)(2,1)} %bitcast.52, f32[8,1,160]{2,1,0:T(1,128)} %broadcast_in_dim.81.weight_ref), custom_call_target="tpu_custom_call" | custom-call | tf_op jit(solution)/shard_map/pallas_call | solution.py:149
  87.3 0.7 reduce
  88.0 0.1 mul.48
  88.1 0.0 copy-done.4
  88.1 0.0 copy-start.7
  88.1 0.0 slice-start
  88.1 4.2 %fusion.6 = f32[1280,256]{0,1:T(8,128)S(1)} fusion(bf16[1280,2048]{1,0:T(8,128)(2,1)} %bitcast.57, bf16[1,2048,256]{2,1,0:T(8,128)(2,1)S(1)} %copy-done.4), kind=kOutput, calls=%fused_computation.25 | convolution fusion | flops 1342177280 | bytes 7602176 | tf_op jit(solution)/shard_map/dot_general | solution.py:324
  92.3 0.0 copy-done
  92.3 0.0 copy-done.7
  92.3 0.0 slice-start.1
  92.4 0.0 copy-start.8
  92.4 1.7 fusion.12
  94.1 0.0 slice-done
  94.1 0.0 slice-done.1
  94.1 0.0 copy-done.8
  94.1 0.0 copy-start.1
  94.1 3.4 %multiply_reduce_fusion = (f32[1280]{0:T(1024)S(1)}, bf16[1280,256]{0,1:T(8,128)(2,1)}, f32[1280,256]{0,1:T(8,128)}) fusion(f32[1280,256]{0,1:T(8,128)S(1)} %fusion.6, f32[1280,256]{0,1:T(8,128)S(1)} %fusion.12, f32[1280]{0:T(1024)S(1)} %mul.48, bf16[1280,2048]{1,0:T(8,128)(2,1)S(1)} %bitcast.63, bf16[1,256,2048]{2,1,0:T(8,128)(2,1)S(1)} %copy-done.8), kind=kOutput, calls=%fused_computation.9 | convolution fusion | flops 1347746560 | bytes 10889216 | tf_op jit(solution)/shard_map/rd,fd->rf/dot_general | solution.py:325
  97.5 0.0 copy-done.1
  97.5 3.2 %convolution_bitcast_fusion = f32[1,256,2048]{2,1,0:T(8,128)} fusion(bf16[1280,2048]{1,0:T(8,128)(2,1)S(1)} %bitcast.64, f32[1280]{0:T(1024)S(1)} %mul.48, f32[1280,256]{0,1:T(8,128)S(1)} %fusion.6, f32[1280,256]{0,1:T(8,128)S(1)} %fusion.12), kind=kOutput, calls=%fused_computation.3 | convolution fusion | flops 1345781760 | bytes 9966592 | tf_op jit(solution)/shard_map/rf,rd->fd/dot_general | solution.py:350
  100.7 0.1 reshape.46.product_ref
  100.8 0.0 copy-start.2
  100.8 0.0 copy-start.3
  100.8 5.7 %convolution_bitcast_fusion.1 = f32[1,2048,256]{2,1,0:T(8,128)} fusion(bf16[1280,2048]{1,0:T(8,128)(2,1)} %bitcast.58, bf16[1280,256]{0,1:T(8,128)(2,1)} %get-tuple-element.16), kind=kOutput, calls=%fused_computation.4 | convolution fusion | flops 1342177280 | bytes 7995392 | tf_op jit(solution)/shard_map/rd,rf->df/dot_general | solution.py:349
  106.5 0.0 copy-done.2
  106.5 0.0 copy-done.3
  106.5 5.7 %convolution_bitcast_fusion.2 = f32[1,2048,256]{2,1,0:T(8,128)} fusion(bf16[1280,2048]{1,0:T(8,128)(2,1)} %bitcast.59, f32[1280,256]{0,1:T(8,128)S(1)} %copy-done.2, f32[1280,256]{0,1:T(8,128)S(1)} %copy-done.3, f32[1280,256]{0,1:T(8,128)S(1)} %fusion.6, f32[1280]{0:T(1024)S(1)} %mul.48), kind=kOutput, calls=%fused_computation.5 | convolution fusion | flops 1348075520 | bytes 11277312 | tf_op jit(solution)/shard_map/rd,rf->df/dot_general | solution.py:348
  112.2 0.0 copy-start.5
  112.2 2.4 %fusion.10 = f32[1280,2048]{1,0:T(8,128)S(1)} fusion(bf16[1,2048,256]{2,1,0:T(8,128)(2,1)S(1)} %copy-done, f32[1280,256]{0,1:T(8,128)S(1)} %copy-done.2, f32[1280,256]{0,1:T(8,128)S(1)} %copy-done.3, f32[1280,256]{0,1:T(8,128)S(1)} %fusion.6, f32[1280]{0:T(1024)S(1)} %mul.48), kind=kOutput, calls=%fused_computation.29 | convolution fusion | flops 1348075520 | bytes 15471616 | tf_op jit(solution)/shard_map/rf,df->rd/dot_general | solution.py:340
  114.7 0.0 copy-done.5
  114.7 3.9 %add_convert_fusion = bf16[1280,2048]{1,0:T(8,128)(2,1)} fusion(f32[1280,2048]{1,0:T(8,128)S(1)} %fusion.10, bf16[1280,256]{0,1:T(8,128)(2,1)S(1)} %copy-done.5, bf16[1,2048,256]{2,1,0:T(8,128)(2,1)S(1)} %copy-done.4), kind=kOutput, calls=%fused_computation | convolution fusion | flops 1347420160 | bytes 17432576 | tf_op jit(solution)/shard_map/rf,df->rd/dot_general | solution.py:341
  118.6 61.1 %shard_map.111 = (bf16[8,160,512]{2,1,0:T(8,128)(2,1)S(1)}, f32[8,1,160]{2,1,0:T(1,128)S(1)}) custom-call(bf16[8,160,2048]{2,1,0:T(8,128)(2,1)} %bitcast.51, f32[8,1,160]{2,1,0:T(1,128)S(1)} %reshape.46.product_ref), custom_call_target="tpu_custom_call" | custom-call | tf_op jit(solution)/shard_map/pallas_call | solution.py:267
  179.7 0.0 copy-start.6
  179.7 1.3 fusion.2
  181.0 0.2 select_reduce_fusion
  181.3 0.0 copy-done.6
  181.3 0.6 select_reduce_fusion.2
  (3 shorter events, 0.0 us)
Async XLA Ops:
  0.6 91.7 %copy-start = (bf16[1,2048,256]{2,1,0:T(8,128)(2,1)S(1)}, bf16[1,2048,256]{2,1,0:T(8,128)(2,1)}, u32[]{:S(2)}) copy-start(bf16[1,2048,256]{2,1,0:T(8,128)(2,1)} %param.11) | copy-start | bytes 3145732
  8.7 79.4 %copy-start.4 = (bf16[1,2048,256]{2,1,0:T(8,128)(2,1)S(1)}, bf16[1,2048,256]{2,1,0:T(8,128)(2,1)}, u32[]{:S(2)}) copy-start(bf16[1,2048,256]{2,1,0:T(8,128)(2,1)} %param.12) | copy-start | bytes 3145732
  88.1 4.3 %copy-start.7 = (bf16[8,160,2048]{2,1,0:T(8,128)(2,1)S(1)}, bf16[8,160,2048]{2,1,0:T(8,128)(2,1)}, u32[]{:S(2)}) copy-start(bf16[8,160,2048]{2,1,0:T(8,128)(2,1)} %get-tuple-element.10) | copy-start | bytes 15728644
  88.1 6.0 %slice-start = ((s8[5242880]{0:T(1024)(128)(4,1)}), s8[4194304]{0:T(1024)(128)(4,1)S(1)}, s32[]{:S(2)}) async-start(s8[5242880]{0:T(1024)(128)(4,1)} %bitcast.61), calls=%async_computation | async-start | bytes 8388608
  92.3 1.7 slice-start.1
  92.4 1.8 copy-start.8
  94.1 3.4 %copy-start.1 = (f32[1280,256]{0,1:T(8,128)}, f32[1280,256]{0,1:T(8,128)S(1)}, u32[]{:S(2)}) copy-start(f32[1280,256]{0,1:T(8,128)S(1)} %fusion.12) | copy-start | bytes 3932164
  100.8 5.7 %copy-start.2 = (f32[1280,256]{0,1:T(8,128)S(1)}, f32[1280,256]{0,1:T(8,128)}, u32[]{:S(2)}) copy-start(f32[1280,256]{0,1:T(8,128)} %copy-done.1) | copy-start | bytes 3932164
  100.8 5.7 %copy-start.3 = (f32[1280,256]{0,1:T(8,128)S(1)}, f32[1280,256]{0,1:T(8,128)}, u32[]{:S(2)}) copy-start(f32[1280,256]{0,1:T(8,128)} %get-tuple-element.17) | copy-start | bytes 3932164
  112.2 2.4 %copy-start.5 = (bf16[1280,256]{0,1:T(8,128)(2,1)S(1)}, bf16[1280,256]{0,1:T(8,128)(2,1)}, u32[]{:S(2)}) copy-start(bf16[1280,256]{0,1:T(8,128)(2,1)} %get-tuple-element.16) | copy-start | bytes 1966084
  179.7 1.5 copy-start.6
